TPU v7x, 32 devices: a whole 2x2x4 slice. The times are simulated.
32 devices in a mesh: kv: 8 (over z, y), tp: 4 (over x, core).
Axes of the slice: x: 2, y: 2, z: 4, core: 2. Of those that a mesh axis runs over, the one named last changes fastest.
Arguments:
- tokens: bfloat16 [16, 3072], P('kv', 'tp'), may hold values from -15 to 15
- associative_state: float32 [16, 16, 128, 128], P('kv', 'tp'), may hold values from -2 to 2
- sudden_extra_decay: float32 [16, 16], P('kv', 'tp'), may hold values from -0.7 to 0
- head_decay_speed: float32 [16], P('tp'), may hold values from 0.05 to 2
- opening_norm_gain: float32 [3072], P('tp'), may hold values from 0.1 to 1.9
- opening_gate_weight: bfloat16 [3072, 8448], P('tp', 'kv'), may hold values from -0.109375 to 0.109375
- opening_up_weight: bfloat16 [3072, 8448], P('tp', 'kv'), may hold values from -0.109375 to 0.109375
- opening_down_weight: bfloat16 [8448, 3072], P('kv', 'tp'), may hold values from -0.25 to 0.25
- mixer_norm_gain: float32 [3072], P('tp'), may hold values from 0.1 to 1.9
- query_matrix: bfloat16 [3072, 2048], P('tp'), may hold values from -0.109375 to 0.109375
- key_matrix: bfloat16 [3072, 2048], P('tp'), may hold values from -0.109375 to 0.109375
- value_matrix: bfloat16 [3072, 2048], P('tp'), may hold values from -0.109375 to 0.109375
- output_gate_matrix: bfloat16 [3072, 2048], P('tp'), may hold values from -0.109375 to 0.109375
- strength_weight: bfloat16 [3072, 16], P('tp'), may hold values from -0.109375 to 0.109375
- decay_matrix: bfloat16 [3072, 16], P('tp'), may hold values from -0.109375 to 0.109375
- head_read_gain: float32 [128], replicated, may hold values from 0.1 to 1.9
- output_matrix: bfloat16 [2048, 3072], P('tp'), may hold values from -0.125 to 0.125
- closing_norm_gain: float32 [3072], P('tp'), may hold values from 0.1 to 1.9
- closing_gate_weight: bfloat16 [3072, 8448], P('tp', 'kv'), may hold values from -0.109375 to 0.109375
- closing_up_weight: bfloat16 [3072, 8448], P('tp', 'kv'), may hold values from -0.109375 to 0.109375
- closing_down_weight: bfloat16 [8448, 3072], P('kv', 'tp'), may hold values from -0.25 to 0.25
Outputs:
- layer_out: bfloat16 [16, 3072], P('kv', 'tp')
- memory_new: float32 [16, 16, 128, 128], P('kv', 'tp')
All inputs are finite; a program needn't handle non-finite values.
Results may differ from a plain program's by a relative error of at most 0.023.
Values may be sent and summed in bfloat16 or wider, within the bound.
A program may use at most 64 MiB of HBM per device.

v0:
```python
import jax
import jax.numpy as jnp
from jax import lax
from jax.sharding import PartitionSpec as P

norm_eps = 1e-06


def feed_forward(resid, rows_in, gain, gate_proj, lift_proj, down_proj):
    model_width = gain.shape[0] * lax.axis_size("tp")
    gathered = lax.all_gather(rows_in, "kv", axis=0, tiled=True)
    values = gathered.astype(jnp.float32)
    scaled = (values * gain).astype(jnp.bfloat16)
    gate_part = jnp.dot(scaled, gate_proj, preferred_element_type=jnp.float32)
    lift_part = jnp.dot(scaled, lift_proj, preferred_element_type=jnp.float32)
    square = jnp.sum(values * values, axis=1)
    gate_sum, lift_sum, square_sum = (
        lax.psum(gate_part.astype(jnp.bfloat16), "tp").astype(jnp.float32),
        lax.psum(lift_part.astype(jnp.bfloat16), "tp").astype(jnp.float32),
        lax.psum(square.astype(jnp.bfloat16), "tp").astype(jnp.float32),
    )
    scale_of_norm = lax.rsqrt(square_sum / model_width + norm_eps)[:, None]
    hidden = (jax.nn.silu(scale_of_norm * gate_sum) * (scale_of_norm * lift_sum)).astype(
        jnp.bfloat16
    )
    down_part = jnp.dot(hidden, down_proj, preferred_element_type=jnp.float32)
    whole_sum = lax.psum(down_part, "kv")
    row_count = resid.shape[0]
    own_rows = lax.dynamic_slice_in_dim(whole_sum, lax.axis_index("kv") * row_count, row_count, 0)
    return resid + 0.5 * own_rows.astype(jnp.bfloat16).astype(jnp.float32)


def unit_norm(values):
    return values * lax.rsqrt(jnp.sum(values * values, axis=-1, keepdims=True) + 1e-12)


def body(
    tokens,
    associative_state,
    sudden_extra_decay,
    head_decay_speed,
    opening_norm_gain,
    opening_gate_weight,
    opening_up_weight,
    opening_down_weight,
    mixer_norm_gain,
    query_matrix,
    key_matrix,
    value_matrix,
    output_gate_matrix,
    strength_weight,
    decay_matrix,
    head_read_gain,
    output_matrix,
    closing_norm_gain,
    closing_gate_weight,
    closing_up_weight,
    closing_down_weight,
):
    model_width = opening_norm_gain.shape[0] * lax.axis_size("tp")
    first = feed_forward(
        tokens.astype(jnp.float32),
        tokens,
        opening_norm_gain,
        opening_gate_weight,
        opening_up_weight,
        opening_down_weight,
    )
    square_sum = lax.psum(jnp.sum(first * first, axis=1), "tp")
    scale_of_norm = lax.rsqrt(square_sum / model_width + norm_eps)[:, None]
    mixer_input = (first * mixer_norm_gain).astype(jnp.bfloat16)
    partials = tuple(
        (
            jnp.dot(mixer_input, weight, preferred_element_type=jnp.float32).astype(jnp.bfloat16)
            for weight in (
                query_matrix,
                key_matrix,
                value_matrix,
                output_gate_matrix,
                strength_weight,
                decay_matrix,
            )
        )
    )
    query_sum, key_sum, value_sum, gate_sum, beta_sum, decay_total = (
        lax.psum_scatter(partials[0], "tp", scatter_dimension=1, tiled=True).astype(jnp.float32),
        lax.psum_scatter(partials[1], "tp", scatter_dimension=1, tiled=True).astype(jnp.float32),
        lax.psum_scatter(partials[2], "tp", scatter_dimension=1, tiled=True).astype(jnp.float32),
        lax.psum_scatter(partials[3], "tp", scatter_dimension=1, tiled=True).astype(jnp.float32),
        lax.psum_scatter(partials[4], "tp", scatter_dimension=1, tiled=True).astype(jnp.float32),
        lax.psum_scatter(partials[5], "tp", scatter_dimension=1, tiled=True).astype(jnp.float32),
    )
    row_count = query_sum.shape[0]
    head_count = head_decay_speed.shape[0]
    head_size = head_read_gain.shape[0]

    def split_heads(values):
        return (scale_of_norm * values).reshape(row_count, head_count, head_size)

    query_vec = unit_norm(split_heads(query_sum)) * head_size ** (-0.5)
    key_vec = unit_norm(split_heads(key_sum))
    value_vec = split_heads(value_sum)
    gate_vec = split_heads(gate_sum)
    beta = jax.nn.sigmoid(scale_of_norm * beta_sum)
    decay_logarithm = (
        -head_decay_speed * jax.nn.softplus(scale_of_norm * decay_total) + sudden_extra_decay
    )
    kept = jnp.exp(decay_logarithm)[:, :, None, None]
    recall = jnp.einsum(
        "bhk,bhkv->bhv", key_vec, associative_state, precision=lax.Precision.HIGHEST
    )
    written = (beta[:, :, None] * key_vec)[:, :, :, None]
    memory_new = (
        kept * (associative_state - written * recall[:, :, None, :])
        + written * value_vec[:, :, None, :]
    )
    read_out = jnp.einsum("bhk,bhkv->bhv", query_vec, memory_new, precision=lax.Precision.HIGHEST)
    normed = read_out * lax.rsqrt(jnp.mean(read_out * read_out, axis=-1, keepdims=True) + norm_eps)
    normed = normed * head_read_gain * jax.nn.silu(gate_vec)
    mix_out = normed.reshape(row_count, head_count * head_size).astype(jnp.bfloat16)
    out_part = jnp.dot(mix_out, output_matrix, preferred_element_type=jnp.float32).astype(
        jnp.bfloat16
    )
    mixed = lax.psum_scatter(out_part, "tp", scatter_dimension=1, tiled=True).astype(jnp.float32)
    second = first + mixed.astype(jnp.bfloat16).astype(jnp.float32)
    final = feed_forward(
        second,
        second.astype(jnp.bfloat16),
        closing_norm_gain,
        closing_gate_weight,
        closing_up_weight,
        closing_down_weight,
    )
    return (final.astype(jnp.bfloat16), memory_new)


def solution(mesh):
    placed = (
        P("kv", "tp"),
        P("kv", "tp", None, None),
        P("kv", "tp"),
        P("tp"),
        P("tp"),
        P("tp", "kv"),
        P("tp", "kv"),
        P("kv", "tp"),
        P("tp"),
        P("tp", None),
        P("tp", None),
        P("tp", None),
        P("tp", None),
        P("tp", None),
        P("tp", None),
        P(),
        P("tp", None),
        P("tp"),
        P("tp", "kv"),
        P("tp", "kv"),
        P("kv", "tp"),
    )
    return jax.shard_map(
        body,
        mesh=mesh,
        in_specs=placed,
        out_specs=(P("kv", "tp"), P("kv", "tp", None, None)),
        check_vma=False,
    )
```

profile of v0, /device:TPU:0, one launch (start us, length us, event | category | flops | bytes accessed | tf_op | source)
XLA Modules:
  0.0 359.4 jit_solution(2355526956701864364)
XLA Ops:
  7.2 32.6 %all-gather = bf16[8,2,768]{2,1,0:T(2,128)(2,1)S(1)} all-gather(bf16[1,2,768]{2,1,0:T(2,128)(2,1)} %bitcast.66), channel_id=1, replica_groups=mesh['kv'=8,'tp'=4] {'kv'}, dimensions={0}, use_global_device_ids=true | all-gather | bytes 27648 | tf_op jit(solution)/shard_map/all_gather | solution.py:11
  40.5 2.6 convolution_convert_fusion.3
  43.2 1.2 convolution_convert_fusion.4
  45.7 29.5 %all-reduce.10.cloned.1.call-done = (bf16[16,1056]{1,0:T(8,128)(2,1)}, bf16[16,1056]{1,0:T(8,128)(2,1)}, bf16[16]{0:T(256)(128)(2,1)}) async-done(((bf16[16,1056]{1,0:T(8,128)(2,1)}, bf16[16,1056]{1,0:T(8,128)(2,1)}, bf16[16]{0:T(256)(128)(2,1)}), (bf16[16,1056]{1,0:T(8,128)(2,1)}, bf16[16,1056]{1,0:T(8,128)(2,1)}, bf16[16]{0:T(256)(128)(2,1)})) %all-reduce.10.cloned.1.call-update) | async-done | bytes 67632 | tf_op jit(solution)/shard_map/psum | solution.py:19
  75.9 1.9 fusion
  77.7 37.9 %psum.66 = bf16[16,768]{1,0:T(8,128)(2,1)S(1)} all-reduce(f32[16,768]{1,0:T(8,128)S(1)} %fusion), channel_id=1, replica_groups=mesh['kv'=8,'tp'=4] {'kv'}, use_global_device_ids=true, to_apply=%region_4.5 | all-reduce | flops 12288 | bytes 73728 | tf_op jit(solution)/shard_map/psum | solution.py:27
  115.8 2.6 convolution_convert_fusion.5
  119.0 1.4 copy-done.2
  122.1 2.4 convolution_convert_fusion.7
  127.0 5.6 %psum.67 = f32[2]{0:T(128)S(1)} all-reduce(f32[2]{0:T(128)S(1)} %get-tuple-element.12), channel_id=1, replica_groups=mesh['kv'=8,'tp'=4] {'tp'}, use_global_device_ids=true, to_apply=%region_6.7 | all-reduce | flops 2 | bytes 16 | tf_op jit(solution)/shard_map/psum | solution.py:69
  133.8 7.8 %all-reduce.3 = (bf16[2,16]{1,0:T(2,128)(2,1)S(1)}, bf16[2,16]{1,0:T(2,128)(2,1)S(1)}) all-reduce(bf16[2,16]{1,0:T(2,128)(2,1)S(1)} %convolution_convert_fusion.9, bf16[2,16]{1,0:T(2,128)(2,1)S(1)} %convolution_convert_fusion.10), channel_id=4, replica_groups=mesh['kv'=8,'tp'=4] {'tp'}, use_global_device_ids=true, to_apply=%region_10.11.clone | all-reduce | flops 64 | bytes 256
  142.7 23.7 %reduce-scatter.20.cloned.1.call-done = bf16[512,2]{1,0:T(8,128)(2,1)} async-done(((bf16[2048,2]{1,0:T(8,128)(2,1)}), bf16[512,2]{1,0:T(8,128)(2,1)}) %reduce-scatter.20.cloned.1.call-update) | async-done | bytes 2064
  167.4 23.0 %reduce-scatter.22.cloned.1.call-done = bf16[512,2]{1,0:T(8,128)(2,1)} async-done(((bf16[2048,2]{1,0:T(8,128)(2,1)}), bf16[512,2]{1,0:T(8,128)(2,1)}) %reduce-scatter.22.cloned.1.call-update) | async-done | bytes 2064
  191.4 23.0 %reduce-scatter.24.cloned.1.call-done = bf16[512,2]{1,0:T(8,128)(2,1)} async-done(((bf16[2048,2]{1,0:T(8,128)(2,1)}), bf16[512,2]{1,0:T(8,128)(2,1)}) %reduce-scatter.24.cloned.1.call-update) | async-done | bytes 2064
  216.0 1.6 fusion.18
  217.6 1.3 multiply_add_fusion
  220.9 1.2 copy.37
  222.2 23.3 %reduce-scatter.26.cloned.1.call-done = bf16[768,2]{1,0:T(8,128)(2,1)} async-done(((bf16[3072,2]{1,0:T(8,128)(2,1)}), bf16[768,2]{1,0:T(8,128)(2,1)}) %reduce-scatter.26.cloned.1.call-update) | async-done | bytes 3088
  246.6 30.6 %all-gather.1 = bf16[8,2,768]{2,1,0:T(2,128)(2,1)S(1)} all-gather(bf16[1,2,768]{2,1,0:T(2,128)(2,1)S(1)} %fusion.9), channel_id=1, replica_groups=mesh['kv'=8,'tp'=4] {'kv'}, dimensions={0}, use_global_device_ids=true | all-gather | bytes 27648 | tf_op jit(solution)/shard_map/all_gather | solution.py:11
  277.9 2.6 convolution_convert_fusion.1
  280.4 1.2 convolution_convert_fusion.2
  281.6 29.9 %all-reduce.8.cloned.1.call-done = (bf16[16,1056]{1,0:T(8,128)(2,1)}, bf16[16,1056]{1,0:T(8,128)(2,1)}, bf16[16]{0:T(256)(128)(2,1)}) async-done(((bf16[16,1056]{1,0:T(8,128)(2,1)}, bf16[16,1056]{1,0:T(8,128)(2,1)}, bf16[16]{0:T(256)(128)(2,1)}), (bf16[16,1056]{1,0:T(8,128)(2,1)}, bf16[16,1056]{1,0:T(8,128)(2,1)}, bf16[16]{0:T(256)(128)(2,1)})) %all-reduce.8.cloned.1.call-update) | async-done | bytes 67632 | tf_op jit(solution)/shard_map/psum | solution.py:19
  312.2 1.9 fusion.1
  314.1 37.9 %psum.71 = bf16[16,768]{1,0:T(8,128)(2,1)S(1)} all-reduce(f32[16,768]{1,0:T(8,128)S(1)} %fusion.1), channel_id=1, replica_groups=mesh['kv'=8,'tp'=4] {'kv'}, use_global_device_ids=true, to_apply=%region_21.22 | all-reduce | flops 12288 | bytes 73728 | tf_op jit(solution)/shard_map/psum | solution.py:27
  (87 shorter events, 17.9 us)
Async XLA Ops:
  7.2 213.2 %copy-start = (bf16[512,3072]{1,0:T(8,128)(2,1)S(1)}, bf16[512,3072]{1,0:T(8,128)(2,1)}, u32[]{:S(2)}) copy-start(bf16[512,3072]{1,0:T(8,128)(2,1)} %param.37) | copy-start | bytes 9437188
  7.2 36.0 %copy-start.7 = (f32[768]{0:T(1024)S(1)}, f32[768]{0:T(1024)}, u32[]{:S(2)}) copy-start(f32[768]{0:T(1024)} %param.25) | copy-start | bytes 9220
  7.2 68.0 %all-reduce.10.cloned.1.call-start = ((), (), s32[]{:S(2)}) async-start(), calls=%async_computation.11 | async-start | bytes 148480 | tf_op jit(solution)/shard_map/psum | solution.py:19
  39.9 3.3 copy-start.4
  40.5 3.9 %copy-start.14 = (f32[4]{0:T(128)S(1)}, f32[4]{0:T(128)}, u32[]{:S(2)}) copy-start(f32[4]{0:T(128)} %param.24) | copy-start | bytes 52
  40.5 3.9 %copy-start.15 = (u32[32]{0:T(128)S(1)}, u32[32]{0:T(128)}, u32[]{:S(2)}) copy-start(u32[32]{0:T(128)} %constant.47) | copy-start | bytes 388
  43.1 72.5 %copy-start.6 = (bf16[2,768]{1,0:T(2,128)(2,1)S(1)}, bf16[2,768]{1,0:T(2,128)(2,1)}, u32[]{:S(2)}) copy-start(bf16[2,768]{1,0:T(2,128)(2,1)} %param.21) | copy-start | bytes 9220
  43.1 72.5 %copy-start.9 = (f32[768]{0:T(1024)S(1)}, f32[768]{0:T(1024)}, u32[]{:S(2)}) copy-start(f32[768]{0:T(1024)} %param.29) | copy-start | bytes 9220
  44.3 97.4 %reduce-scatter.18.cloned.1.call-start = ((), (), s32[]{:S(2)}) async-start(), calls=%async_computation.5 | async-start | bytes 655360
  115.7 2.8 copy-start.1
  118.5 1.9 copy-start.2
  122.0 3.6 %copy-start.12 = (bf16[768,16]{0,1:T(8,128)(2,1)S(1)}, bf16[768,16]{0,1:T(8,128)(2,1)}, u32[]{:S(2)}) copy-start(bf16[768,16]{0,1:T(8,128)(2,1)} %param.34) | copy-start | bytes 73732
  122.0 44.3 %reduce-scatter.20.cloned.1.call-start = ((), (), s32[]{:S(2)}) async-start(), calls=%async_computation.6 | async-start | bytes 655360
  124.5 2.4 copy-start.13
  125.6 90.3 %copy-start.10 = (f32[2,4]{1,0:T(2,128)S(1)}, f32[2,4]{1,0:T(2,128)}, u32[]{:S(2)}) copy-start(f32[2,4]{1,0:T(2,128)} %param.23) | copy-start | bytes 100
  125.6 64.8 %reduce-scatter.22.cloned.1.call-start = ((), (), s32[]{:S(2)}) async-start(), calls=%async_computation.7 | async-start | bytes 655360
  126.8 87.6 %reduce-scatter.24.cloned.1.call-start = ((), (), s32[]{:S(2)}) async-start(), calls=%async_computation.8 | async-start | bytes 655360
  133.7 86.6 %copy-start.11 = (f32[128]{0:T(128)S(1)}, f32[128]{0:T(128)}, u32[]{:S(2)}) copy-start(f32[128]{0:T(128)} %param.36) | copy-start | bytes 1540
  133.8 111.8 %reduce-scatter.26.cloned.1.call-start = ((), (), s32[]{:S(2)}) async-start(), calls=%async_computation.9 | async-start | bytes 983040
  218.9 0.8 copy-start.3
  220.9 57.0 %copy-start.8 = (f32[768]{0:T(1024)S(1)}, f32[768]{0:T(1024)}, u32[]{:S(2)}) copy-start(f32[768]{0:T(1024)} %param.38) | copy-start | bytes 9220
  222.2 89.4 %all-reduce.8.cloned.1.call-start = ((), (), s32[]{:S(2)}) async-start(), calls=%async_computation.10 | async-start | bytes 148480 | tf_op jit(solution)/shard_map/psum | solution.py:19
  277.2 3.2 copy-start.5
Sparse Core Ops, SparseCore 0:
  44.5 30.7 all-reduce.9
  122.1 19.5 reduce-scatter.17
  144.8 21.5 reduce-scatter.19
  168.7 21.6 reduce-scatter.21
  192.7 21.6 reduce-scatter.23
  222.3 23.2 reduce-scatter.25
  281.7 29.7 all-reduce.7
where the time goes:
time: 360 us; the launch traced here: 359 us
  waiting for transfers between devices  153 us (42%)
  blocking collectives  152 us (42%)
  matrix products  20.1 us (6%)
  between operations  15 us (4%)
  local copies, waits for them, and re-layouts  13.6 us (4%)
  other arithmetic  5.3 us (1%)
    unnamed x12, waiting for transfers between devices  93.2 us
    psum x2, blocking collectives, feed_forward(): whole_sum = lax.psum(down_part, 'kv')  75.8 us
    all_gather x2, blocking collectives, feed_forward(): gathered = lax.all_gather(rows_in, 'kv', axis=0, tiled=True)  63.2 us
    psum x2, waiting for transfers between devices, feed_forward(): lax.psum(lift_part.astype(jnp.bfloat16), 'tp').astype(jnp.float32)  59.4 us
    unnamed x43, local copies, waits for them, and re-layouts  13.5 us
    unnamed x1, blocking collectives  7.82 us
  transfers between devices with their start and end apart: 7, of which 7 were waited for; matrix products, arithmetic and copies ran while one was open for 3% of the time, Pallas kernels for 0%

commit v1 on v0

v1 whole, which is shorter than its diff:
```python
import functools

import jax
import jax.numpy as jnp
from jax import lax
from jax.experimental import pallas as pl
from jax.experimental.pallas import tpu as pltpu
from jax.sharding import PartitionSpec as P

norm_eps = 1e-06
MESH = pl.DeviceIdType.MESH
F32, BF16 = jnp.float32, jnp.bfloat16
UNROLL = 16
VMEM_LIMIT = 63 * 1024 * 1024


def each(count, step):
    if count <= UNROLL:
        for i in range(count):
            step(i)
    else:

        def run(i, carry):
            step(i)
            return carry

        lax.fori_loop(0, count, run, 0)


def silu(x):
    return x * jax.nn.sigmoid(x)


def dot_t(rows, weight):
    return lax.dot_general(rows, weight, (((1,), (1,)), ((), ())), preferred_element_type=F32)


class Axis:
    def __init__(self, name, size):
        self.name, self.n, self.me = name, size, lax.axis_index(name)

    def others(self, step):
        each(self.n - 1, lambda i: step(lax.rem(self.me + (i + 1), self.n)))

    def start(self, src_of, land, sems):
        def one(peer):
            pltpu.make_async_remote_copy(
                src_ref=src_of(peer),
                dst_ref=land.at[self.me],
                send_sem=sems.at[0],
                recv_sem=sems.at[1],
                device_id={self.name: peer},
                device_id_type=MESH,
            ).start()

        self.others(one)

    def wait(self, land, sem):
        part = land.at[pl.ds(0, self.n - 1)]
        pltpu.make_async_copy(part, part, sem).wait()


def kernel(
    sizes,
    tokens,
    state_hbm,
    extra,
    speed,
    gain1,
    wg1_hbm,
    wu1_hbm,
    wd1_hbm,
    mgain,
    wq_hbm,
    wk_hbm,
    wv_hbm,
    wz_hbm,
    ws_hbm,
    wa_hbm,
    hgain,
    wo_hbm,
    gain2,
    wg2_hbm,
    wu2_hbm,
    wd2_hbm,
    out,
    new_hbm,
    wg1,
    wu1,
    wd1,
    wq,
    wk,
    wv,
    wz,
    ws,
    wa,
    wo,
    wg2,
    wu2,
    wd2,
    state,
    new,
    u_land,
    rows_scr,
    gate_send,
    gate_land,
    up_send,
    up_land,
    sq_send,
    sq_land,
    hid_send,
    hid_land,
    hid_scr,
    part_send,
    part_land,
    proj_send,
    proj_land,
    small_send,
    small_land,
    mix_send,
    mix_land,
    second_send,
    pair,
    turn,
    head_out,
    load_sem,
    new_sem,
    kv_sem,
    tp_sem,
):
    n_kv, n_tp, heads, head = sizes
    kv, tp = Axis("kv", n_kv), Axis("tp", n_tp)
    rows, width = tokens.shape
    all_rows = rows * n_kv
    group = all_rows // n_tp
    model_width = width * n_tp
    own_width = heads * head
    pairs = rows * heads

    hbm = (wg1_hbm, wu1_hbm, wd1_hbm, wq_hbm, wk_hbm, wv_hbm, wz_hbm, ws_hbm, wa_hbm, state_hbm, wo_hbm, wg2_hbm, wu2_hbm, wd2_hbm)
    local = (wg1, wu1, wd1, wq, wk, wv, wz, ws, wa, state, wo, wg2, wu2, wd2)
    loads = [pltpu.make_async_copy(a, b, load_sem.at[i]) for i, (a, b) in enumerate(zip(hbm, local))]

    barrier = pltpu.get_barrier_semaphore()
    for axis in (kv, tp):
        axis.others(
            lambda peer, axis=axis: pl.semaphore_signal(
                barrier, inc=1, device_id={axis.name: peer}, device_id_type=MESH
            )
        )
    for load in loads:
        load.start()

    pair[...] = jnp.zeros_like(pair)
    turn[...] = jnp.zeros_like(turn)
    for h in range(heads):
        pair[4, rows * h : rows * (h + 1), 0:heads] = extra[...]
    lane = lax.broadcasted_iota(jnp.int32, (pairs, 128), 1)
    head_of = lax.broadcasted_iota(jnp.int32, (pairs, 128), 0) // rows
    own_lane = lane == head_of
    extra_col = jnp.sum(jnp.where(own_lane, pair[4, 0:pairs, 0:128], 0.0), axis=1, keepdims=True)
    pair[5, 0:pairs, 0:heads] = jnp.broadcast_to(speed[...], (pairs, heads))
    speed_col = jnp.sum(jnp.where(own_lane, pair[5, 0:pairs, 0:128], 0.0), axis=1, keepdims=True)

    pl.semaphore_wait(barrier, n_kv - 1 + n_tp - 1)

    def feed_forward(index, resid, src, gain, gate_w, up_w, down_w, load_at):
        land = u_land.at[index]
        kv.start(lambda peer: src, land, kv_sem.at[2 * index])
        u_land[index, kv.me] = src[...]
        kv.wait(land, kv_sem.at[2 * index, 1])

        def place(i):
            rows_scr[rows * i : rows * (i + 1), :] = u_land[index, i].astype(F32)

        for i in range(n_kv):
            place(i)
        values = rows_scr[...]
        scaled = (values * gain[...]).astype(BF16)
        square = jnp.sum(values * values, axis=1, keepdims=True)
        for t in range(n_tp):
            sq_send[index, t] = jnp.broadcast_to(square[group * t : group * (t + 1)], (group, 128))
        tp.start(lambda peer: sq_send.at[index, peer], sq_land.at[index], tp_sem.at[index, 0])
        for place_at, weight, send, landing in ((0, gate_w, gate_send, gate_land), (1, up_w, up_send, up_land)):
            loads[load_at + place_at].wait()
            product = dot_t(scaled, weight[...])
            for t in range(n_tp):
                send[index, t] = product[group * t : group * (t + 1)].astype(BF16)
            tp.start(lambda peer: send.at[index, peer], landing.at[index], tp_sem.at[index, 1 + place_at])

        def total(send, landing, sem):
            landing[index, tp.me] = send[index, tp.me]
            tp.wait(landing.at[index], sem)
            result = landing[index, 0].astype(F32)
            for t in range(1, n_tp):
                result = result + landing[index, t].astype(F32)
            return result

        square = total(sq_send, sq_land, tp_sem.at[index, 0, 1])
        scale = lax.rsqrt(square[:, 0:1] / model_width + norm_eps)
        gate = scale * total(gate_send, gate_land, tp_sem.at[index, 1, 1])
        up = scale * total(up_send, up_land, tp_sem.at[index, 2, 1])
        hidden = (silu(gate) * up).astype(BF16)
        hid_send[index] = hidden
        tp.start(lambda peer: hid_send.at[index], hid_land.at[index], tp_sem.at[index, 3])
        hid_land[index, tp.me] = hidden
        loads[load_at + 2].wait()
        tp.wait(hid_land.at[index], tp_sem.at[index, 3, 1])
        for t in range(n_tp):
            hid_scr[group * t : group * (t + 1), :] = hid_land[index, t].astype(F32)
        rows_scr[...] = jnp.dot(hid_scr[...].astype(BF16), down_w[...], preferred_element_type=F32)

        def cut(i):
            part_send[index, i] = rows_scr[rows * i : rows * (i + 1), :].astype(BF16)

        for i in range(n_kv):
            cut(i)
        kv.start(lambda peer: part_send.at[index, peer], part_land.at[index], kv_sem.at[2 * index + 1])
        part_land[index, kv.me] = part_send[index, kv.me]
        kv.wait(part_land.at[index], kv_sem.at[2 * index + 1, 1])
        if n_kv <= UNROLL:
            branch = part_land[index, 0].astype(F32)
            for i in range(1, n_kv):
                branch = branch + part_land[index, i].astype(F32)
        else:
            branch = lax.fori_loop(
                0, n_kv, lambda i, c: c + part_land[index, i].astype(F32), jnp.zeros((rows, width), F32)
            )
        return resid + 0.5 * branch.astype(BF16).astype(F32)

    first = feed_forward(0, tokens[...].astype(F32), tokens, gain1, wg1, wu1, wd1, 0)

    mixer_in = (first * mgain[...]).astype(BF16)
    square = jnp.sum(first * first, axis=1, keepdims=True)
    for w, weight in enumerate((wq, wk, wv, wz)):
        loads[3 + w].wait()
        product = jnp.dot(mixer_in, weight[...], preferred_element_type=F32)
        for t in range(n_tp):
            proj_send[w, t] = product[:, own_width * t : own_width * (t + 1)].astype(BF16)
        tp.start(lambda peer: proj_send.at[w, peer], proj_land.at[w], tp_sem.at[2, w])
    loads[7].wait()
    loads[8].wait()
    all_heads = ws.shape[0]
    small_send[...] = jnp.zeros_like(small_send)
    small_send[:, 0:all_heads] = dot_t(mixer_in, ws[...])
    small_send[:, 128 : 128 + all_heads] = dot_t(mixer_in, wa[...])
    small_send[:, 256:384] = jnp.broadcast_to(square, (rows, 128))
    tp.start(lambda peer: small_send, small_land, tp_sem.at[3, 0])
    small_land[tp.me] = small_send[...]
    for w in range(4):
        proj_land[w, tp.me] = proj_send[w, tp.me]
    loads[9].wait()
    loads[10].wait()
    for w in range(4):
        tp.wait(proj_land.at[w], tp_sem.at[2, w, 1])
    tp.wait(small_land, tp_sem.at[3, 0, 1])
    small = small_land[0]
    for t in range(1, n_tp):
        small = small + small_land[t]
    scale = lax.rsqrt(small[:, 256:257] / model_width + norm_eps)
    small = scale * small
    for w in range(4):
        value = proj_land[w, 0].astype(F32)
        for t in range(1, n_tp):
            value = value + proj_land[w, t].astype(F32)
        value = scale * value
        for h in range(heads):
            pair[w, rows * h : rows * (h + 1), :] = value[:, head * h : head * (h + 1)]
    for h in range(heads):
        pair[4, rows * h : rows * (h + 1), 0:128] = small[:, 0:128]
        pair[5, rows * h : rows * (h + 1), 0:128] = small[:, 128:256]
    my_lane = lane == head_of + heads * tp.me
    beta = jax.nn.sigmoid(jnp.sum(jnp.where(my_lane, pair[4, 0:pairs, 0:128], 0.0), axis=1, keepdims=True))
    decay = jnp.sum(jnp.where(my_lane, pair[5, 0:pairs, 0:128], 0.0), axis=1, keepdims=True)
    softplus = jnp.maximum(decay, 0.0) + jnp.log1p(jnp.exp(-jnp.abs(decay)))
    kept = jnp.exp(extra_col - speed_col * softplus)
    query, key = pair[0, 0:pairs, :], pair[1, 0:pairs, :]
    query = query * lax.rsqrt(jnp.sum(query * query, axis=1, keepdims=True) + 1e-12) * head ** (-0.5)
    key = key * lax.rsqrt(jnp.sum(key * key, axis=1, keepdims=True) + 1e-12)
    value, gate = pair[2, 0:pairs, :], pair[3, 0:pairs, :]
    overlap = jnp.sum(query * key, axis=1, keepdims=True)
    turn[0:pairs, :] = key
    turn[pairs : 2 * pairs, :] = query
    columns = jnp.transpose(turn[...])
    for p in range(pairs):
        h, r = p // rows, p % rows
        block = state[r, h]
        key_col, query_col = columns[:, p : p + 1], columns[:, pairs + p : pairs + p + 1]
        keep = kept[p : p + 1]
        recall = jnp.sum(key_col * block, axis=0, keepdims=True)
        seen = jnp.sum(query_col * block, axis=0, keepdims=True)
        delta = beta[p : p + 1] * (value[p : p + 1] - keep * recall)
        new[r, h] = keep * block + key_col * delta
        pair[6, p : p + 1, :] = keep * seen + overlap[p : p + 1] * delta
    save = pltpu.make_async_copy(new, new_hbm, new_sem)
    save.start()
    read = pair[6, 0:pairs, :]
    normed = read * lax.rsqrt(jnp.mean(read * read, axis=1, keepdims=True) + norm_eps)
    pair[6, 0:pairs, :] = normed * hgain[...] * silu(gate)
    for h in range(heads):
        head_out[:, head * h : head * (h + 1)] = pair[6, rows * h : rows * (h + 1), :]
    product = jnp.dot(head_out[...].astype(BF16), wo[...], preferred_element_type=F32)
    for t in range(n_tp):
        mix_send[t] = product[:, width * t : width * (t + 1)].astype(BF16)
    tp.start(lambda peer: mix_send.at[peer], mix_land, tp_sem.at[3, 1])
    mix_land[tp.me] = mix_send[tp.me]
    tp.wait(mix_land, tp_sem.at[3, 1, 1])
    mixed = mix_land[0].astype(F32)
    for t in range(1, n_tp):
        mixed = mixed + mix_land[t].astype(F32)
    second = first + mixed.astype(BF16).astype(F32)
    second_send[...] = second.astype(BF16)

    final = feed_forward(1, second, second_send, gain2, wg2, wu2, wd2, 11)
    out[...] = final.astype(BF16)

    save.wait()
    for index in range(2):
        kv.wait(u_land.at[index], kv_sem.at[2 * index, 0])
        kv.wait(part_land.at[index], kv_sem.at[2 * index + 1, 0])
        for i, landing in enumerate((sq_land, gate_land, up_land, hid_land)):
            tp.wait(landing.at[index], tp_sem.at[index, i, 0])
    for w in range(4):
        tp.wait(proj_land.at[w], tp_sem.at[2, w, 0])
    tp.wait(small_land, tp_sem.at[3, 0, 0])
    tp.wait(mix_land, tp_sem.at[3, 1, 0])


def body(n_kv, n_tp, *args):
    tokens, state, extra, speed = args[:4]
    wg, wd, wq, ws, wo = args[5], args[7], args[9], args[13], args[16]
    hgain = args[15]
    rows, width = tokens.shape
    heads, head = speed.shape[0], hgain.shape[0]
    hidden = wg.shape[1]
    own_width = heads * head
    all_rows = rows * n_kv
    group = all_rows // n_tp
    pair_rows = -(-rows * heads // 8) * 8
    args = [a.reshape(1, -1) if a.ndim == 1 else a for a in args]
    for i in (5, 6, 13, 14, 18, 19):
        args[i] = args[i].T
    vmem, anywhere = pl.BlockSpec(memory_space=pltpu.VMEM), pl.BlockSpec(memory_space=pl.ANY)
    in_vmem = {0, 2, 3, 4, 8, 15, 17}
    scratch = [
        pltpu.VMEM(a.shape, a.dtype)
        for a in (args[5], args[6], args[7], *args[9:15], args[16], *args[18:21], state, state)
    ]
    scratch += [
        pltpu.VMEM((2, n_kv, rows, width), BF16),
        pltpu.VMEM((all_rows, width), F32),
        pltpu.VMEM((2, n_tp, group, hidden), BF16),
        pltpu.VMEM((2, n_tp, group, hidden), BF16),
        pltpu.VMEM((2, n_tp, group, hidden), BF16),
        pltpu.VMEM((2, n_tp, group, hidden), BF16),
        pltpu.VMEM((2, n_tp, group, 128), F32),
        pltpu.VMEM((2, n_tp, group, 128), F32),
        pltpu.VMEM((2, group, hidden), BF16),
        pltpu.VMEM((2, n_tp, group, hidden), BF16),
        pltpu.VMEM((all_rows, hidden), F32),
        pltpu.VMEM((2, n_kv, rows, width), BF16),
        pltpu.VMEM((2, n_kv, rows, width), BF16),
        pltpu.VMEM((4, n_tp, rows, own_width), BF16),
        pltpu.VMEM((4, n_tp, rows, own_width), BF16),
        pltpu.VMEM((rows, 384), F32),
        pltpu.VMEM((n_tp, rows, 384), F32),
        pltpu.VMEM((n_tp, rows, width), BF16),
        pltpu.VMEM((n_tp, rows, width), BF16),
        pltpu.VMEM((rows, width), BF16),
        pltpu.VMEM((7, pair_rows, head), F32),
        pltpu.VMEM((128, head), F32),
        pltpu.VMEM((rows, own_width), F32),
        pltpu.SemaphoreType.DMA((14,)),
        pltpu.SemaphoreType.DMA,
        pltpu.SemaphoreType.DMA((4, 2)),
        pltpu.SemaphoreType.DMA((4, 4, 2)),
    ]
    return pl.pallas_call(
        functools.partial(kernel, (n_kv, n_tp, heads, head)),
        out_shape=(
            jax.ShapeDtypeStruct(tokens.shape, BF16),
            jax.ShapeDtypeStruct(state.shape, F32),
        ),
        in_specs=[vmem if i in in_vmem else anywhere for i in range(len(args))],
        out_specs=(vmem, anywhere),
        scratch_shapes=scratch,
        compiler_params=pltpu.CompilerParams(
            collective_id=0, has_side_effects=True, vmem_limit_bytes=VMEM_LIMIT
        ),
    )(*args)


def solution(mesh):
    placed = (
        P("kv", "tp"),
        P("kv", "tp", None, None),
        P("kv", "tp"),
        P("tp"),
        P("tp"),
        P("tp", "kv"),
        P("tp", "kv"),
        P("kv", "tp"),
        P("tp"),
        P("tp", None),
        P("tp", None),
        P("tp", None),
        P("tp", None),
        P("tp", None),
        P("tp", None),
        P(),
        P("tp", None),
        P("tp"),
        P("tp", "kv"),
        P("tp", "kv"),
        P("kv", "tp"),
    )
    return jax.shard_map(
        functools.partial(body, mesh.shape["kv"], mesh.shape["tp"]),
        mesh=mesh,
        in_specs=placed,
        out_specs=(P("kv", "tp"), P("kv", "tp", None, None)),
        check_vma=False,
    )
```

time: 360 us -> 54.9 us (0.15)
  waiting for transfers between devices: 153 us -> 0 us
  blocking collectives: 152 us -> 0 us
  Pallas kernels: 0 us -> 47 us
  matrix products: 20.1 us -> 0 us
  between operations: 15 us -> 0.64 us
  local copies, waits for them, and re-layouts: 13.6 us -> 6.94 us
  other arithmetic: 5.3 us -> 0 us
    unnamed x12 -> x0, waiting for transfers between devices: 93.2 us -> none
    psum x3 -> x0, blocking collectives: 81.5 us -> none  [the longest x2 75.8 us: feed_forward(): whole_sum = lax.psum(down_part, 'kv')]
    all_gather x2 -> x0, blocking collectives: 63.2 us -> none  [feed_forward(): gathered = lax.all_gather(rows_in, 'kv', axis=0, tiled=True)]
    psum x2 -> x0, waiting for transfers between devices: 59.4 us -> none  [feed_forward(): lax.psum(lift_part.astype(jnp.bfloat16), 'tp').astype(jnp.float32)]
    pallas_call x0 -> x1, Pallas kernels: none -> 47 us  [body(): pl.pallas_call(functools.partial(kernel, (n_kv, n_tp, heads, head)), out_...]
    dot_general x15 -> x0, matrix products: 20.1 us -> none  [the longest x6 6.24 us: body(): jnp.dot(mixer_input, weight, preferred_element_type=jnp.float32)]
    unnamed x43 -> x2, local copies, waits for them, and re-layouts: 13.5 us -> 3.14 us
    unnamed x1 -> x0, blocking collectives: 7.82 us -> none
  transfers between devices with their start and end apart: 7 -> 0, of which waited for: 7 -> 0; matrix products, arithmetic and copies ran while one was open for 3% -> 0% of each run, Pallas kernels for 0% -> 0%
where the time goes in v1:
time: 54.9 us; the launch traced here: 54.6 us
  Pallas kernels  47 us (86%)
  local copies, waits for them, and re-layouts  6.94 us (13%)
  between operations  0.64 us (1%)
    pallas_call x1, Pallas kernels, body(): pl.pallas_call(functools.partial(kernel, (n_kv, n_tp, heads, head)), out_...  47 us
    reshape x3, local copies, waits for them, and re-layouts, body(): args = [a.reshape(1, -1) if a.ndim == 1 else a for a in args]  3.8 us
    unnamed x2, local copies, waits for them, and re-layouts  3.14 us

profile of v1, /device:TPU:0, one launch (start us, length us, event | category | flops | bytes accessed | tf_op | source)
XLA Modules:
  0.0 54.6 jit_solution(15485854051579105561)
XLA Ops:
  0.6 1.3 %reshape.20.gain1 = f32[1,768]{1,0:T(1,128)} reshape(f32[768]{0:T(1024)} %param.25) | data formatting | bytes 6144 | tf_op jit(solution)/shard_map/reshape | solution.py:340
  1.9 1.3 %reshape.21.mgain = f32[1,768]{1,0:T(1,128)} reshape(f32[768]{0:T(1024)} %param.29) | data formatting | bytes 6144 | tf_op jit(solution)/shard_map/reshape | solution.py:340
  3.2 1.3 %reshape.23.gain2 = f32[1,768]{1,0:T(1,128)} reshape(f32[768]{0:T(1024)} %param.38) | data formatting | bytes 6144 | tf_op jit(solution)/shard_map/reshape | solution.py:340
  4.4 47.0 %shard_map.212 = (bf16[2,768]{1,0:T(2,128)(2,1)}, f32[2,4,128,128]{3,2,1,0:T(8,128)}) custom-call(bf16[2,768]{1,0:T(2,128)(2,1)} %tokens.1, f32[2,4,128,128]{3,2,1,0:T(8,128)} %state_hbm.1, f32[2,4]{1,0:T(2,128)} %extra.1, f32[1,4]{1,0:T(1,128)} %bitcast.14, f32[1,768]{1,0:T(1,128)} %reshape.20.gain1, bf16[1056,768]{1,0:T(8,128)(2,1)} %bitcast.8, ...), custom_call_target="tpu_custom_call" | custom-call | tf_op jit(solution)/shard_map/pallas_call | solution.py:378
  51.4 1.3 %copy.25 = bf16[2,768]{1,0:T(2,128)(2,1)} copy(bf16[2,768]{1,0:T(2,128)(2,1)} %get-tuple-element.4) | data formatting | bytes 6144
  52.7 1.9 %copy.26 = f32[2,4,128,128]{3,2,1,0:T(8,128)} copy(f32[2,4,128,128]{3,2,1,0:T(8,128)} %get-tuple-element.5) | data formatting | bytes 1048576

commit v2 on v1

--- a/solution.py
+++ b/solution.py
@@ -38,6 +38,7 @@
 class Axis:
     def __init__(self, name, size):
         self.name, self.n, self.me = name, size, lax.axis_index(name)
+        self.sent = []
 
     def others(self, step):
         each(self.n - 1, lambda i: step(lax.rem(self.me + (i + 1), self.n)))
@@ -54,6 +55,7 @@
             ).start()
 
         self.others(one)
+        self.sent.append((land, sems.at[0]))
 
     def wait(self, land, sem):
         part = land.at[pl.ds(0, self.n - 1)]
@@ -102,14 +104,14 @@
     new,
     u_land,
     rows_scr,
-    gate_send,
-    gate_land,
-    up_send,
-    up_land,
+    pair_send,
+    pair_land,
+    chip_send,
+    chip_land,
     sq_send,
     sq_land,
-    hid_send,
-    hid_land,
+    sq_chip_send,
+    sq_chip_land,
     hid_scr,
     part_send,
     part_land,
@@ -123,16 +125,21 @@
     pair,
     turn,
     head_out,
+    gains,
     load_sem,
     new_sem,
     kv_sem,
     tp_sem,
+    mate_sem,
 ):
     n_kv, n_tp, heads, head = sizes
     kv, tp = Axis("kv", n_kv), Axis("tp", n_tp)
     rows, width = tokens.shape
     all_rows = rows * n_kv
-    group = all_rows // n_tp
+    half = all_rows // 2
+    core = lax.rem(tp.me, 2)
+    mate = tp.me + 1 - 2 * core
+    to_finish = []
     model_width = width * n_tp
     own_width = heads * head
     pairs = rows * heads
@@ -148,9 +155,13 @@
                 barrier, inc=1, device_id={axis.name: peer}, device_id_type=MESH
             )
         )
-    for load in loads:
+    for load in loads[0:2]:
         load.start()
 
+    for i, gain in enumerate((gain1, mgain, gain2)):
+        lanes = gain.shape[1]
+        for j in range(gain.shape[0]):
+            gains[i, :, lanes * j : lanes * (j + 1)] = gain[j : j + 1, :]
     pair[...] = jnp.zeros_like(pair)
     turn[...] = jnp.zeros_like(turn)
     for h in range(heads):
@@ -163,11 +174,17 @@
     speed_col = jnp.sum(jnp.where(own_lane, pair[5, 0:pairs, 0:128], 0.0), axis=1, keepdims=True)
 
     pl.semaphore_wait(barrier, n_kv - 1 + n_tp - 1)
+    stages = [loads[2:5], loads[5:11], loads[11:14]]
+
+    def next_stage():
+        for load in stages.pop(0) if stages else ():
+            load.start()
 
     def feed_forward(index, resid, src, gain, gate_w, up_w, down_w, load_at):
         land = u_land.at[index]
         kv.start(lambda peer: src, land, kv_sem.at[2 * index])
         u_land[index, kv.me] = src[...]
+        next_stage()
         kv.wait(land, kv_sem.at[2 * index, 1])
 
         def place(i):
@@ -175,39 +192,61 @@
 
         for i in range(n_kv):
             place(i)
+        next_stage()
         values = rows_scr[...]
-        scaled = (values * gain[...]).astype(BF16)
+        scaled = (values * gain).astype(BF16)
         square = jnp.sum(values * values, axis=1, keepdims=True)
-        for t in range(n_tp):
-            sq_send[index, t] = jnp.broadcast_to(square[group * t : group * (t + 1)], (group, 128))
-        tp.start(lambda peer: sq_send.at[index, peer], sq_land.at[index], tp_sem.at[index, 0])
-        for place_at, weight, send, landing in ((0, gate_w, gate_send, gate_land), (1, up_w, up_send, up_land)):
-            loads[load_at + place_at].wait()
-            product = dot_t(scaled, weight[...])
-            for t in range(n_tp):
-                send[index, t] = product[group * t : group * (t + 1)].astype(BF16)
-            tp.start(lambda peer: send.at[index, peer], landing.at[index], tp_sem.at[index, 1 + place_at])
-
-        def total(send, landing, sem):
-            landing[index, tp.me] = send[index, tp.me]
-            tp.wait(landing.at[index], sem)
-            result = landing[index, 0].astype(F32)
-            for t in range(1, n_tp):
-                result = result + landing[index, t].astype(F32)
+        def to_mate(which, product, send, landing):
+            for c in range(2):
+                send[index, which, c] = product[half * c : half * (c + 1)].astype(send.dtype)
+            copy = pltpu.make_async_remote_copy(
+                src_ref=send.at[index, which, 1 - core],
+                dst_ref=landing.at[index, which],
+                send_sem=mate_sem.at[index, which + (send is sq_send) * 2, 0],
+                recv_sem=mate_sem.at[index, which + (send is sq_send) * 2, 1],
+                device_id={tp.name: mate},
+                device_id_type=MESH,
+            )
+            copy.start()
+            to_finish.append(copy)
+            return copy
+
+        def to_all(which, copy, send, landing, chip_send, chip_land):
+            copy.wait_recv()
+            chip = send[index, which, core].astype(F32) + landing[index, which].astype(F32)
+            chip_send[index, which] = chip.astype(chip_send.dtype)
+            tp.start(
+                lambda peer: chip_send.at[index, which],
+                chip_land.at[index, which],
+                tp_sem.at[index, which + (send is sq_send) * 2],
+            )
+            chip_land[index, which, tp.me] = chip.astype(chip_send.dtype)
+
+        square_copy = to_mate(0, jnp.broadcast_to(square, (all_rows, 128)), sq_send, sq_land)
+        loads[load_at].wait()
+        gate_copy = to_mate(0, dot_t(scaled, gate_w[...]), pair_send, pair_land)
+        loads[load_at + 1].wait()
+        up_part = dot_t(scaled, up_w[...])
+        up_copy = to_mate(1, up_part, pair_send, pair_land)
+        to_all(0, square_copy, sq_send, sq_land, sq_chip_send, sq_chip_land)
+        to_all(0, gate_copy, pair_send, pair_land, chip_send, chip_land)
+        to_all(1, up_copy, pair_send, pair_land, chip_send, chip_land)
+        next_stage()
+        loads[load_at + 2].wait()
+        tp.wait(sq_chip_land.at[index, 0], tp_sem.at[index, 2, 1])
+        tp.wait(chip_land.at[index, 0], tp_sem.at[index, 0, 1])
+        tp.wait(chip_land.at[index, 1], tp_sem.at[index, 1, 1])
+
+        def total(landing, which, c):
+            result = landing[index, which, c].astype(F32)
+            for t in range(c + 2, n_tp, 2):
+                result = result + landing[index, which, t].astype(F32)
             return result
 
-        square = total(sq_send, sq_land, tp_sem.at[index, 0, 1])
-        scale = lax.rsqrt(square[:, 0:1] / model_width + norm_eps)
-        gate = scale * total(gate_send, gate_land, tp_sem.at[index, 1, 1])
-        up = scale * total(up_send, up_land, tp_sem.at[index, 2, 1])
-        hidden = (silu(gate) * up).astype(BF16)
-        hid_send[index] = hidden
-        tp.start(lambda peer: hid_send.at[index], hid_land.at[index], tp_sem.at[index, 3])
-        hid_land[index, tp.me] = hidden
-        loads[load_at + 2].wait()
-        tp.wait(hid_land.at[index], tp_sem.at[index, 3, 1])
-        for t in range(n_tp):
-            hid_scr[group * t : group * (t + 1), :] = hid_land[index, t].astype(F32)
+        for c in range(2):
+            scale = lax.rsqrt(total(sq_chip_land, 0, c)[:, 0:1] / model_width + norm_eps)
+            gate, up = scale * total(chip_land, 0, c), scale * total(chip_land, 1, c)
+            hid_scr[half * c : half * (c + 1), :] = silu(gate) * up
         rows_scr[...] = jnp.dot(hid_scr[...].astype(BF16), down_w[...], preferred_element_type=F32)
 
         def cut(i):
@@ -228,9 +267,9 @@
             )
         return resid + 0.5 * branch.astype(BF16).astype(F32)
 
-    first = feed_forward(0, tokens[...].astype(F32), tokens, gain1, wg1, wu1, wd1, 0)
-
-    mixer_in = (first * mgain[...]).astype(BF16)
+    first = feed_forward(0, tokens[...].astype(F32), tokens, gains[0], wg1, wu1, wd1, 0)
+
+    mixer_in = (first * gains[1]).astype(BF16)
     square = jnp.sum(first * first, axis=1, keepdims=True)
     for w, weight in enumerate((wq, wk, wv, wz)):
         loads[3 + w].wait()
@@ -311,19 +350,28 @@
     second = first + mixed.astype(BF16).astype(F32)
     second_send[...] = second.astype(BF16)
 
-    final = feed_forward(1, second, second_send, gain2, wg2, wu2, wd2, 11)
+    final = feed_forward(1, second, second_send, gains[2], wg2, wu2, wd2, 11)
     out[...] = final.astype(BF16)
 
     save.wait()
-    for index in range(2):
-        kv.wait(u_land.at[index], kv_sem.at[2 * index, 0])
-        kv.wait(part_land.at[index], kv_sem.at[2 * index + 1, 0])
-        for i, landing in enumerate((sq_land, gate_land, up_land, hid_land)):
-            tp.wait(landing.at[index], tp_sem.at[index, i, 0])
-    for w in range(4):
-        tp.wait(proj_land.at[w], tp_sem.at[2, w, 0])
-    tp.wait(small_land, tp_sem.at[3, 0, 0])
-    tp.wait(mix_land, tp_sem.at[3, 1, 0])
+    for copy in to_finish:
+        copy.wait_send()
+    for axis in (kv, tp):
+        for landing, sem in axis.sent:
+            axis.wait(landing, sem)
+
+
+def hand_over(out_in, new_in, out, new, held, in_sem, out_sem):
+    reads = [pltpu.make_async_copy(new_in.at[r], held.at[r], in_sem.at[r]) for r in range(held.shape[0])]
+    writes = [pltpu.make_async_copy(held.at[r], new.at[r], out_sem.at[r]) for r in range(held.shape[0])]
+    for read in reads:
+        read.start()
+    out[...] = out_in[...]
+    for read, write in zip(reads, writes):
+        read.wait()
+        write.start()
+    for write in writes:
+        write.wait()
 
 
 def body(n_kv, n_tp, *args):
@@ -335,9 +383,9 @@
     hidden = wg.shape[1]
     own_width = heads * head
     all_rows = rows * n_kv
-    group = all_rows // n_tp
+    half = all_rows // 2
     pair_rows = -(-rows * heads // 8) * 8
-    args = [a.reshape(1, -1) if a.ndim == 1 else a for a in args]
+    args = [a.reshape(-1, 128 if a.size % 128 == 0 else a.size) if a.ndim == 1 else a for a in args]
     for i in (5, 6, 13, 14, 18, 19):
         args[i] = args[i].T
     vmem, anywhere = pl.BlockSpec(memory_space=pltpu.VMEM), pl.BlockSpec(memory_space=pl.ANY)
@@ -349,14 +397,14 @@
     scratch += [
         pltpu.VMEM((2, n_kv, rows, width), BF16),
         pltpu.VMEM((all_rows, width), F32),
-        pltpu.VMEM((2, n_tp, group, hidden), BF16),
-        pltpu.VMEM((2, n_tp, group, hidden), BF16),
-        pltpu.VMEM((2, n_tp, group, hidden), BF16),
-        pltpu.VMEM((2, n_tp, group, hidden), BF16),
-        pltpu.VMEM((2, n_tp, group, 128), F32),
-        pltpu.VMEM((2, n_tp, group, 128), F32),
-        pltpu.VMEM((2, group, hidden), BF16),
-        pltpu.VMEM((2, n_tp, group, hidden), BF16),
+        pltpu.VMEM((2, 2, 2, half, hidden), BF16),
+        pltpu.VMEM((2, 2, half, hidden), BF16),
+        pltpu.VMEM((2, 2, half, hidden), BF16),
+        pltpu.VMEM((2, 2, n_tp, half, hidden), BF16),
+        pltpu.VMEM((2, 1, 2, half, 128), F32),
+        pltpu.VMEM((2, 1, half, 128), F32),
+        pltpu.VMEM((2, 1, half, 128), F32),
+        pltpu.VMEM((2, 1, n_tp, half, 128), F32),
         pltpu.VMEM((all_rows, hidden), F32),
         pltpu.VMEM((2, n_kv, rows, width), BF16),
         pltpu.VMEM((2, n_kv, rows, width), BF16),
@@ -370,12 +418,14 @@
         pltpu.VMEM((7, pair_rows, head), F32),
         pltpu.VMEM((128, head), F32),
         pltpu.VMEM((rows, own_width), F32),
+        pltpu.VMEM((3, 1, width), F32),
         pltpu.SemaphoreType.DMA((14,)),
         pltpu.SemaphoreType.DMA,
         pltpu.SemaphoreType.DMA((4, 2)),
         pltpu.SemaphoreType.DMA((4, 4, 2)),
+        pltpu.SemaphoreType.DMA((2, 3, 2)),
     ]
-    return pl.pallas_call(
+    out, new = pl.pallas_call(
         functools.partial(kernel, (n_kv, n_tp, heads, head)),
         out_shape=(
             jax.ShapeDtypeStruct(tokens.shape, BF16),
@@ -388,6 +438,21 @@
             collective_id=0, has_side_effects=True, vmem_limit_bytes=VMEM_LIMIT
         ),
     )(*args)
+    return pl.pallas_call(
+        hand_over,
+        out_shape=(
+            jax.ShapeDtypeStruct(tokens.shape, BF16),
+            jax.ShapeDtypeStruct(state.shape, F32),
+        ),
+        in_specs=[vmem, anywhere],
+        out_specs=(vmem, anywhere),
+        scratch_shapes=[
+            pltpu.VMEM(state.shape, F32),
+            pltpu.SemaphoreType.DMA((rows,)),
+            pltpu.SemaphoreType.DMA((rows,)),
+        ],
+        compiler_params=pltpu.CompilerParams(vmem_limit_bytes=VMEM_LIMIT),
+    )(out, new)
 
 
 def solution(mesh):

time: 54.9 us -> 48.3 us (0.88)
  local copies, waits for them, and re-layouts: 6.94 us -> 0 us
    reshape x3 -> x0, local copies, waits for them, and re-layouts: 3.8 us -> none  [body(): args = [a.reshape(1, -1) if a.ndim == 1 else a for a in args]]
    unnamed x2 -> x0, local copies, waits for them, and re-layouts: 3.14 us -> none
    pallas_call x0 -> x1, Pallas kernels: none -> 3.02 us  [body(): pl.pallas_call(hand_over, out_shape=(jax.ShapeDtypeStruct(tokens.shape, B...]
    pallas_call x1, Pallas kernels: 47 us -> 44.4 us  [body(): pl.pallas_call(functools.partial(kernel, (n_kv, n_tp, heads, head)), out_...]
where the time goes in v2:
time: 48.3 us; the launch traced here: 48.1 us
  Pallas kernels  47.4 us (98%)
  between operations  0.65 us (1%)
    pallas_call x1, Pallas kernels, body(): pl.pallas_call(functools.partial(kernel, (n_kv, n_tp, heads, head)), out_...  44.4 us
    pallas_call x1, Pallas kernels, body(): pl.pallas_call(hand_over, out_shape=(jax.ShapeDtypeStruct(tokens.shape, B...  3.02 us

profile of v2, /device:TPU:0, one launch (start us, length us, event | category | flops | bytes accessed | tf_op | source)
XLA Modules:
  0.0 48.1 jit_solution(2633462137412518085)
XLA Ops:
  0.6 44.4 %shard_map.212 = (bf16[2,768]{1,0:T(2,128)(2,1)}, f32[2,4,128,128]{3,2,1,0:T(8,128)}) custom-call(bf16[2,768]{1,0:T(2,128)(2,1)} %tokens.1, f32[2,4,128,128]{3,2,1,0:T(8,128)} %state_hbm.1, f32[2,4]{1,0:T(2,128)} %extra.1, f32[1,4]{1,0:T(1,128)} %bitcast.20, f32[6,128]{1,0:T(8,128)} %bitcast.17, bf16[1056,768]{1,0:T(8,128)(2,1)} %bitcast.11, ...), custom_call_target="tpu_custom_call" | custom-call | tf_op jit(solution)/shard_map/pallas_call | solution.py:428
  45.1 3.0 %shard_map.213 = (bf16[2,768]{1,0:T(2,128)(2,1)}, f32[2,4,128,128]{3,2,1,0:T(8,128)}) custom-call(bf16[2,768]{1,0:T(2,128)(2,1)} %get-tuple-element.4.out_in, f32[2,4,128,128]{3,2,1,0:T(8,128)} %get-tuple-element.5.new_in), custom_call_target="tpu_custom_call" | custom-call | tf_op jit(solution)/shard_map/pallas_call | solution.py:441
